TPU v7x, 256 devices: a whole 4x4x8 slice. The times are simulated.
256 devices in a mesh: ep: 64 (over z, y, core), tp: 4 (over x).
Axes of the slice: x: 4, y: 4, z: 8, core: 2. Of those that a mesh axis runs over, the one named last changes fastest.
Arguments:
- mixer_in: bfloat16 [32768, 4096], P(('ep', 'tp')), may hold values from -6 to 6
- mixer_gain: float32 [4096], replicated, may hold values from 0.1 to 1.9
- group_weight: bfloat16 [4, 1024, 1024], P('tp'), may hold values from -0.1875 to 0.1875
- group_scale: float32 [4, 1024], P('tp'), may hold values from 0.1 to 1.9
- expert_in: bfloat16 [32768, 4096], P(('ep', 'tp')), may hold values from -6 to 6
- expert_gain: float32 [4096], replicated, may hold values from 0.1 to 1.9
- routes: int32 [32768, 2], P('ep'), may hold values from 0 to 63, all different within a row; in each aligned block of 128 rows (0 to 127, 128 to 255, ...) at most 6 rows name the same one
- route_weight: float32 [32768, 2], P('ep'), may hold values from 0.2 to 1
- gate_weight: bfloat16 [64, 4096, 1024], P('ep', None, 'tp'), may hold values from -0.25 to 0.25
- up_weight: bfloat16 [64, 4096, 1024], P('ep', None, 'tp'), may hold values from -0.25 to 0.25
- down_weight: bfloat16 [64, 1024, 4096], P('ep', 'tp'), may hold values from -0.02734375 to 0.02734375
Outputs:
- mixed: bfloat16 [32768, 4096], P('ep', 'tp')
- expert_out: bfloat16 [32768, 4096], P(('ep', 'tp'))
Inputs may be any that keep to these rules, and one draw needn't show every extreme that they name: `routes`: each row names 2 different experts; within the rows of one device (aligned blocks of 128 rows) no expert is named more than 6 times, and that count is reached.
All inputs are finite; a program needn't handle non-finite values.
Results may differ from a plain program's by a relative error of at most 0.012.
Values may be sent and summed in bfloat16 or wider, within the bound.
A program may use at most 128 MiB of HBM per device.

v0:
```python
import jax
import jax.numpy as jnp
from jax import lax
from jax.sharding import PartitionSpec as P

WMAX = 16
TOP = 2
epsilon = 1e-06
clamp_limit = 7.0
sigmoid_slope = 1.702


def from_behind(x, axis, by):
    count = lax.axis_size(axis)
    pairs = [(i, i + by) for i in range(count) if 0 <= i + by < count]
    return lax.ppermute(x, axis, pairs)


def rms_norm(values, gain):
    widened = values.astype(jnp.float32)
    scaled = widened * lax.rsqrt(jnp.mean(widened * widened, axis=-1, keepdims=True) + epsilon)
    return (scaled * gain).astype(jnp.bfloat16)


def clamped_unit(gate_part, up_part):
    gate_part = jnp.minimum(gate_part, clamp_limit)
    up_part = jnp.clip(up_part, -clamp_limit, clamp_limit)
    return ((up_part + 1.0) * gate_part * jax.nn.sigmoid(sigmoid_slope * gate_part)).astype(
        jnp.bfloat16
    )


def slot_table(block_routes, experts, capacity):
    count = block_routes.shape[0]
    onehot = (
        block_routes[:, :, None] == jnp.arange(experts, dtype=jnp.int32)[None, None, :]
    ).astype(jnp.int32)
    per_token = jnp.sum(onehot, axis=1)
    earlier = jnp.cumsum(per_token, axis=0) - per_token
    slot_rank = jnp.sum(onehot * earlier[:, None, :], axis=2)
    matches = onehot[:, :, :, None] * (
        slot_rank[:, :, None, None] == jnp.arange(capacity, dtype=jnp.int32)[None, None, None, :]
    ).astype(jnp.int32)
    source = jnp.sum(matches * jnp.arange(count, dtype=jnp.int32)[:, None, None, None], axis=(0, 1))
    filled = jnp.sum(matches, axis=(0, 1))
    return (source, filled, slot_rank)


def shards(
    mixer_in,
    mixer_gain,
    group_weight,
    group_scale,
    expert_in,
    expert_gain,
    routes,
    route_weight,
    gate_weight,
    up_weight,
    down_weight,
):
    normed = rms_norm(mixer_in, mixer_gain)
    shard_rows = lax.all_to_all(normed, "tp", split_axis=1, concat_axis=0, tiled=True)
    length = shard_rows.shape[0]
    last_rows = shard_rows[length - (WMAX - 1) :]
    before = from_behind(last_rows, "ep", 1)
    extended = jnp.concatenate([before, shard_rows], axis=0).astype(jnp.float32)
    window = 2 << lax.axis_index("tp")
    position = lax.axis_index("ep") * length + jnp.arange(length, dtype=jnp.int32)
    prefix = jnp.concatenate(
        [jnp.zeros((1, extended.shape[1]), jnp.float32), jnp.cumsum(extended, axis=0)], axis=0
    )
    upper = prefix[WMAX:]
    lower = lax.dynamic_slice_in_dim(prefix, WMAX - window, length, 0)
    counts = jnp.minimum(position + 1, window).astype(jnp.float32)[:, None]
    pooled = ((upper - lower) / counts - extended[WMAX - 1 :]).astype(jnp.bfloat16)
    mixed = (
        jnp.dot(pooled, group_weight[0], preferred_element_type=jnp.float32) * group_scale[0]
    ).astype(jnp.bfloat16)
    expert_norm = rms_norm(expert_in, expert_gain)
    tok_count = expert_in.shape[0]
    width = expert_in.shape[1]
    experts = lax.axis_size("ep")
    capacity = max(2, 3 * tok_count * TOP // (2 * experts))
    tp_index = lax.axis_index("tp")
    own_routes = lax.dynamic_slice_in_dim(routes, tp_index * tok_count, tok_count, 0)
    own_weight = lax.dynamic_slice_in_dim(route_weight, tp_index * tok_count, tok_count, 0)
    gate_local = gate_weight[0]
    up_local = up_weight[0]
    source, filled, own_rank = slot_table(own_routes, experts, capacity)
    outgoing = expert_norm[source] * filled[:, :, None].astype(jnp.bfloat16)
    arrived = lax.all_to_all(outgoing, "ep", split_axis=0, concat_axis=0, tiled=True)
    piece = lax.all_gather(arrived.reshape(-1, width), "tp", axis=0, tiled=True)
    hidden = clamped_unit(
        jnp.dot(piece, gate_local, preferred_element_type=jnp.float32),
        jnp.dot(piece, up_local, preferred_element_type=jnp.float32),
    )
    down_local = down_weight[0]
    part_width = down_local.shape[0]
    unit_block = lax.all_to_all(hidden, "tp", split_axis=0, concat_axis=1, tiled=True)
    empty = jnp.zeros((unit_block.shape[0], width), jnp.float32)
    total = empty
    piece = lax.all_gather(down_local, "tp", axis=0, tiled=True)
    for part in range(piece.shape[0] // part_width):
        columns = lax.dynamic_slice_in_dim(unit_block, part * part_width, part_width, 1)
        partial_value = jnp.dot(
            columns,
            piece[part * part_width : (part + 1) * part_width],
            preferred_element_type=jnp.float32,
        ).astype(jnp.bfloat16)
        total = total + lax.optimization_barrier(partial_value).astype(jnp.float32)
    summed = total
    summed = summed.astype(jnp.bfloat16).reshape(experts, capacity, width)
    returned = lax.all_to_all(summed, "ep", split_axis=0, concat_axis=0, tiled=True)
    flat_rows = returned.reshape(-1, width)
    slot_index = own_routes * capacity + own_rank
    expert_sum = jnp.zeros((tok_count, width), jnp.float32)
    for choice_slot in range(TOP):
        expert_sum = (
            expert_sum
            + flat_rows[slot_index[:, choice_slot]].astype(jnp.float32)
            * own_weight[:, choice_slot : choice_slot + 1]
        )
    return (mixed, expert_sum.astype(jnp.bfloat16))


def solution(mesh):
    in_specs = (
        P(("ep", "tp"), None),
        P(),
        P("tp", None, None),
        P("tp", None),
        P(("ep", "tp"), None),
        P(),
        P("ep", None),
        P("ep", None),
        P("ep", None, "tp"),
        P("ep", None, "tp"),
        P("ep", "tp", None),
    )
    out_specs = (P("ep", "tp"), P(("ep", "tp"), None))
    return jax.shard_map(shards, mesh=mesh, in_specs=in_specs, out_specs=out_specs, check_vma=False)
```

profile of v0, /device:TPU:96, one launch (start us, length us, event | category | flops | bytes accessed | tf_op | source)
XLA Modules:
  0.0 527.5 jit_solution(16319428711208255795)
XLA Ops:
  12.1 4.1 gather_fusion
  16.2 5.7 %reshape.101 = bf16[64,6,4096]{2,1,0:T(8,128)(2,1)} reshape(bf16[384,4096]{1,0:T(8,128)(2,1)} %gather_fusion) | data formatting | bytes 6291456 | tf_op jit(solution)/shard_map/gather | solution.py:91
  24.5 105.1 %all_to_all.48 = bf16[64,6,4096]{2,1,0:T(8,128)(2,1)} all-to-all(bf16[64,6,4096]{2,1,0:T(8,128)(2,1)S(1)} %broadcast_multiply_fusion), channel_id=1, replica_groups=mesh['ep'=64,'tp'=4] {'ep'}, dimensions={0} | all-to-all | bytes 6291456 | tf_op jit(solution)/shard_map/all_to_all | solution.py:92
  129.7 5.7 %reshape.97 = bf16[384,4096]{1,0:T(8,128)(2,1)} reshape(bf16[64,6,4096]{2,1,0:T(8,128)(2,1)} %all_to_all.48) | data formatting | bytes 6291456 | tf_op jit(solution)/shard_map/reshape | solution.py:93
  138.4 116.5 %all-gather.4.cloned.1.call-done = bf16[1536,4096]{1,0:T(8,128)(2,1)} async-done(((bf16[384,4096]{1,0:T(8,128)(2,1)}), bf16[1536,4096]{1,0:T(8,128)(2,1)}) %all-gather.4.cloned.1.call-update) | async-done | bytes 12582928 | tf_op jit(solution)/shard_map/all_gather | solution.py:93
  254.9 7.7 %convolution_minimum_fusion = f32[1536,256]{1,0:T(8,128)S(1)} fusion(bf16[1536,4096]{1,0:T(8,128)(2,1)} %all-gather.4.cloned.1.call-done, bf16[1,4096,256]{2,1,0:T(8,128)(2,1)} %param.19), kind=kOutput, calls=%fused_computation.10 | convolution fusion | flops 3221618688 | bytes 16252928 | tf_op jit(solution)/shard_map/dot_general | solution.py:95
  264.3 4.9 fusion.5
  271.6 4.2 all-to-all-start.2
  277.3 20.3 %all-to-all-done.2 = bf16[4,384,256]{1,2,0:T(8,128)(2,1)} async-done(((bf16[4,384,256]{1,2,0:T(8,128)(2,1)}), bf16[4,384,256]{1,2,0:T(8,128)(2,1)}, u32[]{:S(2)}, u32[]{:S(2)}) %all-to-all-start.2) | async-done | bytes 786464 | tf_op jit(solution)/shard_map/all_to_all | solution.py:100
  297.6 3.7 all-to-all-start
  301.3 61.7 %all-gather.6.cloned.1.call-done = bf16[1,1024,4096]{2,1,0:T(8,128)(2,1)} async-done(((bf16[1,256,4096]{2,1,0:T(8,128)(2,1)}), bf16[1,1024,4096]{2,1,0:T(8,128)(2,1)}) %all-gather.6.cloned.1.call-update) | async-done | bytes 8388624 | tf_op jit(solution)/shard_map/all_gather | solution.py:103
  363.0 2.8 convolution_convert_fusion.3
  365.8 3.0 convolution_convert_fusion.2
  372.7 4.1 add_convert_fusion
  376.8 5.7 %reshape.98 = bf16[64,6,4096]{2,1,0:T(8,128)(2,1)} reshape(bf16[384,4096]{1,0:T(8,128)(2,1)} %add_convert_fusion) | data formatting | bytes 6291456 | tf_op jit(solution)/shard_map/reshape | solution.py:113
  383.5 10.5 %all-to-all-start.3 = ((bf16[64,6,4096]{2,1,0:T(8,128)(2,1)}), bf16[64,6,4096]{2,1,0:T(8,128)(2,1)}, u32[]{:S(2)}, u32[]{:S(2)}) async-start(bf16[64,6,4096]{2,1,0:T(8,128)(2,1)} %reshape.98), calls=%async_computation.3 | async-start | bytes 8388608 | tf_op jit(solution)/shard_map/all_to_all | solution.py:114
  399.2 88.1 %collective-permute-done = bf16[15,1024]{1,0:T(8,128)(2,1)S(1)} collective-permute-done((bf16[15,1024]{1,0:T(8,128)(2,1)S(1)}, bf16[15,1024]{1,0:T(8,128)(2,1)S(1)}, u32[]{:S(2)}, u32[]{:S(2)}) %collective-permute-start) | collective-permute-done | bytes 30752 | tf_op jit(solution)/shard_map/ppermute | solution.py:16
  489.3 2.6 fusion
  493.9 2.6 broadcast_add_fusion
  499.7 2.6 multiply_convert_fusion
  502.3 5.7 %reshape.99 = bf16[384,4096]{1,0:T(8,128)(2,1)} reshape(bf16[64,6,4096]{2,1,0:T(8,128)(2,1)} %all-to-all-done.3) | data formatting | bytes 6291456 | tf_op jit(solution)/shard_map/reshape | solution.py:115
  508.0 4.5 gather_fusion.1
  512.5 5.5 %gather_fusion.2 = bf16[128,4096]{1,0:T(8,128)(2,1)} fusion(bf16[384,4096]{1,0:T(8,128)(2,1)} %reshape.99, s32[1024]{0:T(1024)S(1)} %get-tuple-element.10), kind=kCustom, calls=%fused_computation.2 | custom fusion | bytes 2097664 | tf_op jit(solution)/shard_map/gather | solution.py:121
  518.0 2.7 add_convert_fusion.1
  (66 shorter events, 33.1 us)
Async XLA Ops:
  7.2 491.2 %copy-start = (bf16[1,1024,1024]{2,1,0:T(8,128)(2,1)S(1)}, bf16[1,1024,1024]{2,1,0:T(8,128)(2,1)}, u32[]{:S(2)}) copy-start(bf16[1,1024,1024]{2,1,0:T(8,128)(2,1)} %param.13) | copy-start | bytes 6291460
  7.2 247.7 %all-gather.4.cloned.1.call-start = ((), (), s32[]{:S(2)}) async-start(), calls=%async_computation.4 | async-start | bytes 15728640 | tf_op jit(solution)/shard_map/all_gather | solution.py:93
  135.4 227.6 %all-gather.6.cloned.1.call-start = ((), (), s32[]{:S(2)}) async-start(), calls=%async_computation.5 | async-start | bytes 10485760 | tf_op jit(solution)/shard_map/all_gather | solution.py:103
  254.9 8.8 %copy-start.6 = (bf16[1536,4096]{1,0:T(8,128)(2,1)S(1)}, bf16[1536,4096]{1,0:T(8,128)(2,1)}, u32[]{:S(2)}) copy-start(bf16[1536,4096]{1,0:T(8,128)(2,1)} %all-gather.4.cloned.1.call-done) | copy-start | bytes 37748740
  254.9 9.4 %copy-start.7 = (bf16[1,4096,256]{2,1,0:T(8,128)(2,1)S(1)}, bf16[1,4096,256]{2,1,0:T(8,128)(2,1)}, u32[]{:S(2)}) copy-start(bf16[1,4096,256]{2,1,0:T(8,128)(2,1)} %param.20) | copy-start | bytes 6291460
  269.2 6.6 %copy-start.5 = (f32[4096]{0:T(1024)S(1)}, f32[4096]{0:T(1024)}, u32[]{:S(2)}) copy-start(f32[4096]{0:T(1024)} %param.12) | copy-start | bytes 49156
  271.6 26.0 %all-to-all-start.2 = ((bf16[4,384,256]{1,2,0:T(8,128)(2,1)}), bf16[4,384,256]{1,2,0:T(8,128)(2,1)}, u32[]{:S(2)}, u32[]{:S(2)}) async-start(bf16[4,384,256]{1,2,0:T(8,128)(2,1)} %copy.36), calls=%async_computation.2 | async-start | bytes 1572864 | tf_op jit(solution)/shard_map/all_to_all | solution.py:100
  297.6 84.9 %all-to-all-start = ((bf16[128,4,1024]{0,2,1:T(8,128)(2,1)}), bf16[128,4,1024]{0,2,1:T(8,128)(2,1)S(1)}, u32[]{:S(2)}, u32[]{:S(2)}) async-start(bf16[128,4,1024]{0,2,1:T(8,128)(2,1)} %bitcast.59), calls=%async_computation | async-start | bytes 2097152 | tf_op jit(solution)/shard_map/all_to_all | solution.py:63
  363.0 5.8 %copy-start.2 = (bf16[1,1024,4096]{2,1,0:T(8,128)(2,1)S(1)}, bf16[1,1024,4096]{2,1,0:T(8,128)(2,1)}, u32[]{:S(2)}) copy-start(bf16[1,1024,4096]{2,1,0:T(8,128)(2,1)} %all-gather.6.cloned.1.call-done) | copy-start | bytes 25165828
  382.5 1.0 copy-start.3
  383.5 118.8 %all-to-all-start.3 = ((bf16[64,6,4096]{2,1,0:T(8,128)(2,1)}), bf16[64,6,4096]{2,1,0:T(8,128)(2,1)}, u32[]{:S(2)}, u32[]{:S(2)}) async-start(bf16[64,6,4096]{2,1,0:T(8,128)(2,1)} %reshape.98), calls=%async_computation.3 | async-start | bytes 8388608 | tf_op jit(solution)/shard_map/all_to_all | solution.py:114
  396.9 90.4 %collective-permute-start = (bf16[15,1024]{1,0:T(8,128)(2,1)S(1)}, bf16[15,1024]{1,0:T(8,128)(2,1)S(1)}, u32[]{:S(2)}, u32[]{:S(2)}) collective-permute-start(bf16[15,1024]{1,0:T(8,128)(2,1)S(1)} %slice.67), channel_id=1, source_target_pairs={{0,4},{4,8},{8,12},{12,16},{16,20},{20,24},{24,28},{28,32},{32,36}... | collective-permute-start | bytes 92168 | tf_op jit(solution)/shard_map/ppermute | solution.py:16
  491.9 2.0 copy-start.1
  498.0 1.6 copy-start.4
  498.1 1.6 copy-start.8
Sparse Core Ops, SparseCore 0:
  135.5 119.3 all-gather.3
  256.7 106.2 all-gather.5
where the time goes:
time: 529 us; the launch traced here: 528 us
  waiting for transfers between devices  287 us (54%)
  blocking collectives  105 us (20%)
  local copies, waits for them, and re-layouts  52.3 us (10%)
  matrix products  25 us (5%)
  other arithmetic  22.6 us (4%)
  starting transfers between devices  20.8 us (4%)
  between operations  14.3 us (3%)
    all_gather x1, waiting for transfers between devices, shards(): piece = lax.all_gather(arrived.reshape(-1, width), 'tp', axis=0, tiled=True)  117 us
    all_to_all x1, blocking collectives, shards(): lax.all_to_all(outgoing, 'ep', split_axis=0, concat_axis=0, tiled=True)  105 us
    ppermute x1, waiting for transfers between devices, from_behind(): return lax.ppermute(x, axis, pairs)  88.1 us
    all_gather x1, waiting for transfers between devices, shards(): piece = lax.all_gather(down_local, 'tp', axis=0, tiled=True)  61.7 us
    all_to_all x1, waiting for transfers between devices, shards(): lax.all_to_all(hidden, 'tp', split_axis=0, concat_axis=1, tiled=True)  20.3 us
  transfers between devices with their start and end apart: 6, of which 4 were waited for; matrix products, arithmetic and copies ran while one was open for 10% of the time, Pallas kernels for 0%

commit v1 on v0

--- a/solution.py
+++ b/solution.py
@@ -100,7 +100,9 @@
     unit_block = lax.all_to_all(hidden, "tp", split_axis=0, concat_axis=1, tiled=True)
     empty = jnp.zeros((unit_block.shape[0], width), jnp.float32)
     total = empty
-    piece = lax.all_gather(down_local, "tp", axis=0, tiled=True)
+    piece = jnp.concatenate(
+        lax.all_to_all(jnp.stack([down_local] * lax.axis_size("tp")), "tp", 0, 0), axis=0
+    )
     for part in range(piece.shape[0] // part_width):
         columns = lax.dynamic_slice_in_dim(unit_block, part * part_width, part_width, 1)
         partial_value = jnp.dot(

time: 529 us -> 544 us (1.028)
  local copies, waits for them, and re-layouts: 52.3 us -> 58.2 us
    all_gather x1, waiting for transfers between devices: 117 us -> 192 us  [shards(): piece = lax.all_gather(arrived.reshape(-1, width), 'tp', axis=0, tiled=True)]
    all_gather x1 -> x0, waiting for transfers between devices: 61.7 us -> none  [shards(): piece = lax.all_gather(down_local, 'tp', axis=0, tiled=True)]
    all_to_all x1, waiting for transfers between devices: 20.3 us -> 11.2 us  [shards(): lax.all_to_all(hidden, 'tp', split_axis=0, concat_axis=1, tiled=True)]
    another operation x3 -> x4, local copies, waits for them, and re-layouts: 1.77 us -> 7.7 us  [the longest x1 5.93 us: shards(): jnp.stack([down_local] * lax.axis_size('tp'))]
    all_to_all x0 -> x1, starting transfers between devices: none -> 5.66 us  [shards(): lax.all_to_all(jnp.stack([down_local] * lax.axis_size('tp')), 'tp', 0, 0)]
  transfers between devices with their start and end apart: 6 -> 6, of which waited for: 4 -> 3; matrix products, arithmetic and copies ran while one was open for 10% -> 11% of each run, Pallas kernels for 0% -> 0%
where the time goes in v1:
time: 544 us; the launch traced here: 542 us
  waiting for transfers between devices  291 us (53%)
  blocking collectives  105 us (19%)
  local copies, waits for them, and re-layouts  58.2 us (11%)
  matrix products  26.2 us (5%)
  starting transfers between devices  24.3 us (4%)
  other arithmetic  22.6 us (4%)
  between operations  14.3 us (3%)
    all_gather x1, waiting for transfers between devices, shards(): piece = lax.all_gather(arrived.reshape(-1, width), 'tp', axis=0, tiled=True)  192 us
    all_to_all x1, blocking collectives, shards(): lax.all_to_all(outgoing, 'ep', split_axis=0, concat_axis=0, tiled=True)  105 us
    ppermute x1, waiting for transfers between devices, from_behind(): return lax.ppermute(x, axis, pairs)  88.1 us
    all_to_all x1, waiting for transfers between devices, shards(): lax.all_to_all(hidden, 'tp', split_axis=0, concat_axis=1, tiled=True)  11.2 us
  transfers between devices with their start and end apart: 6, of which 3 were waited for; matrix products, arithmetic and copies ran while one was open for 11% of the time, Pallas kernels for 0%

profile of v1, /device:TPU:96, one launch (start us, length us, event | category | flops | bytes accessed | tf_op | source)
XLA Modules:
  0.0 541.9 jit_solution(8709757876134757399)
XLA Ops:
  12.1 4.1 gather_fusion
  16.2 5.6 %reshape.107 = bf16[64,6,4096]{2,1,0:T(8,128)(2,1)} reshape(bf16[384,4096]{1,0:T(8,128)(2,1)} %gather_fusion) | data formatting | bytes 6291456 | tf_op jit(solution)/shard_map/gather | solution.py:91
  24.5 105.1 %all_to_all.53 = bf16[64,6,4096]{2,1,0:T(8,128)(2,1)} all-to-all(bf16[64,6,4096]{2,1,0:T(8,128)(2,1)S(1)} %broadcast_multiply_fusion), channel_id=1, replica_groups=mesh['ep'=64,'tp'=4] {'ep'}, dimensions={0} | all-to-all | bytes 6291456 | tf_op jit(solution)/shard_map/all_to_all | solution.py:92
  129.6 5.7 %reshape.103 = bf16[384,4096]{1,0:T(8,128)(2,1)} reshape(bf16[64,6,4096]{2,1,0:T(8,128)(2,1)} %all_to_all.53) | data formatting | bytes 6291456 | tf_op jit(solution)/shard_map/reshape | solution.py:93
  135.4 5.9 %stack.3 = bf16[4,256,4096]{2,1,0:T(8,128)(2,1)} broadcast(bf16[256,4096]{1,0:T(8,128)(2,1)} %bitcast.62), dimensions={1,2} | broadcast | bytes 10485760 | tf_op jit(solution)/shard_map/stack | solution.py:104
  141.3 5.7 %all-to-all-start.3 = ((bf16[4,256,4096]{2,1,0:T(8,128)(2,1)}), bf16[4,256,4096]{2,1,0:T(8,128)(2,1)}, u32[]{:S(2)}, u32[]{:S(2)}) async-start(bf16[4,256,4096]{2,1,0:T(8,128)(2,1)} %stack.3), calls=%async_computation.3 | async-start | bytes 16777216 | tf_op jit(solution)/shard_map/all_to_all | solution.py:104
  149.2 191.8 %all-gather.2.cloned.1.call-done = bf16[1536,4096]{1,0:T(8,128)(2,1)} async-done(((bf16[384,4096]{1,0:T(8,128)(2,1)}), bf16[1536,4096]{1,0:T(8,128)(2,1)}) %all-gather.2.cloned.1.call-update) | async-done | bytes 12582928 | tf_op jit(solution)/shard_map/all_gather | solution.py:93
  341.0 7.7 %convolution_minimum_fusion = f32[1536,256]{1,0:T(8,128)S(1)} fusion(bf16[1536,4096]{1,0:T(8,128)(2,1)} %all-gather.2.cloned.1.call-done, bf16[1,4096,256]{2,1,0:T(8,128)(2,1)} %param.19), kind=kOutput, calls=%fused_computation.10 | convolution fusion | flops 3221618688 | bytes 16252928 | tf_op jit(solution)/shard_map/dot_general | solution.py:95
  350.4 4.9 fusion.5
  357.6 4.2 all-to-all-start.2
  363.3 11.2 %all-to-all-done.2 = bf16[4,384,256]{1,2,0:T(8,128)(2,1)} async-done(((bf16[4,384,256]{1,2,0:T(8,128)(2,1)}), bf16[4,384,256]{1,2,0:T(8,128)(2,1)}, u32[]{:S(2)}, u32[]{:S(2)}) %all-to-all-start.2) | async-done | bytes 786464 | tf_op jit(solution)/shard_map/all_to_all | solution.py:100
  374.6 3.7 all-to-all-start
  378.3 2.7 convolution_convert_fusion.3
  381.0 2.7 convolution_convert_fusion.2
  383.7 2.7 convolution_convert_fusion.1
  386.5 2.7 convolution_convert_fusion
  389.2 4.1 add_convert_fusion
  393.3 5.6 %reshape.104 = bf16[64,6,4096]{2,1,0:T(8,128)(2,1)} reshape(bf16[384,4096]{1,0:T(8,128)(2,1)} %add_convert_fusion) | data formatting | bytes 6291456 | tf_op jit(solution)/shard_map/reshape | solution.py:115
  399.9 8.4 %all-to-all-start.4 = ((bf16[64,6,4096]{2,1,0:T(8,128)(2,1)}), bf16[64,6,4096]{2,1,0:T(8,128)(2,1)}, u32[]{:S(2)}, u32[]{:S(2)}) async-start(bf16[64,6,4096]{2,1,0:T(8,128)(2,1)} %reshape.104), calls=%async_computation.4 | async-start | bytes 8388608 | tf_op jit(solution)/shard_map/all_to_all | solution.py:116
  413.6 88.1 %collective-permute-done = bf16[15,1024]{1,0:T(8,128)(2,1)S(1)} collective-permute-done((bf16[15,1024]{1,0:T(8,128)(2,1)S(1)}, bf16[15,1024]{1,0:T(8,128)(2,1)S(1)}, u32[]{:S(2)}, u32[]{:S(2)}) %collective-permute-start) | collective-permute-done | bytes 30752 | tf_op jit(solution)/shard_map/ppermute | solution.py:16
  516.6 5.7 %reshape.105 = bf16[384,4096]{1,0:T(8,128)(2,1)} reshape(bf16[64,6,4096]{2,1,0:T(8,128)(2,1)} %all-to-all-done.4) | data formatting | bytes 6291456 | tf_op jit(solution)/shard_map/reshape | solution.py:117
  522.4 4.5 gather_fusion.1
  526.9 5.5 %gather_fusion.2 = bf16[128,4096]{1,0:T(8,128)(2,1)} fusion(bf16[384,4096]{1,0:T(8,128)(2,1)} %reshape.105, s32[1024]{0:T(1024)S(1)} %get-tuple-element.10), kind=kCustom, calls=%fused_computation.2 | custom fusion | bytes 2097664 | tf_op jit(solution)/shard_map/gather | solution.py:123
  532.3 2.7 add_convert_fusion.1
  (64 shorter events, 36.3 us)
Async XLA Ops:
  7.2 505.5 %copy-start = (bf16[1,1024,1024]{2,1,0:T(8,128)(2,1)S(1)}, bf16[1,1024,1024]{2,1,0:T(8,128)(2,1)}, u32[]{:S(2)}) copy-start(bf16[1,1024,1024]{2,1,0:T(8,128)(2,1)} %param.13) | copy-start | bytes 6291460
  7.2 333.9 %all-gather.2.cloned.1.call-start = ((), (), s32[]{:S(2)}) async-start(), calls=%async_computation.5 | async-start | bytes 15728640 | tf_op jit(solution)/shard_map/all_gather | solution.py:93
  141.3 216.3 %all-to-all-start.3 = ((bf16[4,256,4096]{2,1,0:T(8,128)(2,1)}), bf16[4,256,4096]{2,1,0:T(8,128)(2,1)}, u32[]{:S(2)}, u32[]{:S(2)}) async-start(bf16[4,256,4096]{2,1,0:T(8,128)(2,1)} %stack.3), calls=%async_computation.3 | async-start | bytes 16777216 | tf_op jit(solution)/shard_map/all_to_all | solution.py:104
  341.0 8.8 %copy-start.5 = (bf16[1536,4096]{1,0:T(8,128)(2,1)S(1)}, bf16[1536,4096]{1,0:T(8,128)(2,1)}, u32[]{:S(2)}) copy-start(bf16[1536,4096]{1,0:T(8,128)(2,1)} %all-gather.2.cloned.1.call-done) | copy-start | bytes 37748740
  341.0 9.4 %copy-start.6 = (bf16[1,4096,256]{2,1,0:T(8,128)(2,1)S(1)}, bf16[1,4096,256]{2,1,0:T(8,128)(2,1)}, u32[]{:S(2)}) copy-start(bf16[1,4096,256]{2,1,0:T(8,128)(2,1)} %param.20) | copy-start | bytes 6291460
  355.3 6.5 %copy-start.4 = (f32[4096]{0:T(1024)S(1)}, f32[4096]{0:T(1024)}, u32[]{:S(2)}) copy-start(f32[4096]{0:T(1024)} %param.12) | copy-start | bytes 49156
  357.6 16.9 %all-to-all-start.2 = ((bf16[4,384,256]{1,2,0:T(8,128)(2,1)}), bf16[4,384,256]{1,2,0:T(8,128)(2,1)}, u32[]{:S(2)}, u32[]{:S(2)}) async-start(bf16[4,384,256]{1,2,0:T(8,128)(2,1)} %copy.36), calls=%async_computation.2 | async-start | bytes 1572864 | tf_op jit(solution)/shard_map/all_to_all | solution.py:100
  374.6 24.4 %all-to-all-start = ((bf16[128,4,1024]{0,2,1:T(8,128)(2,1)}), bf16[128,4,1024]{0,2,1:T(8,128)(2,1)S(1)}, u32[]{:S(2)}, u32[]{:S(2)}) async-start(bf16[128,4,1024]{0,2,1:T(8,128)(2,1)} %bitcast.60), calls=%async_computation | async-start | bytes 2097152 | tf_op jit(solution)/shard_map/all_to_all | solution.py:63
  399.0 1.0 copy-start.2
  399.9 116.7 %all-to-all-start.4 = ((bf16[64,6,4096]{2,1,0:T(8,128)(2,1)}), bf16[64,6,4096]{2,1,0:T(8,128)(2,1)}, u32[]{:S(2)}, u32[]{:S(2)}) async-start(bf16[64,6,4096]{2,1,0:T(8,128)(2,1)} %reshape.104), calls=%async_computation.4 | async-start | bytes 8388608 | tf_op jit(solution)/shard_map/all_to_all | solution.py:116
  411.3 90.4 %collective-permute-start = (bf16[15,1024]{1,0:T(8,128)(2,1)S(1)}, bf16[15,1024]{1,0:T(8,128)(2,1)S(1)}, u32[]{:S(2)}, u32[]{:S(2)}) collective-permute-start(bf16[15,1024]{1,0:T(8,128)(2,1)S(1)} %slice.79), channel_id=1, source_target_pairs={{0,4},{4,8},{8,12},{12,16},{16,20},{20,24},{24,28},{28,32},{32,36}... | collective-permute-start | bytes 92168 | tf_op jit(solution)/shard_map/ppermute | solution.py:16
  506.2 2.0 copy-start.1
  512.4 1.6 copy-start.3
  512.4 1.6 copy-start.7
Sparse Core Ops, SparseCore 0:
  135.5 205.5 all-gather.1
